TPU v7x, 32 devices: a whole 2x2x4 slice. The times are simulated.
32 devices in a mesh: rep: 2 (over x), fs: 4 (over z), tp: 4 (over y, core).
Axes of the slice: x: 2, y: 2, z: 4, core: 2. Of those that a mesh axis runs over, the one named last changes fastest.
Arguments:
- tokens: bfloat16 [4096, 2048], P(('rep', 'fs', 'tp')), may hold values from -6 to 6
- mix_gain: bfloat16 [2048], replicated, may hold values from 0.099609375 to 1.8984375
- gate_proj: bfloat16 [2048, 512], P('fs', 'tp'), may hold values from -0.125 to 0.125
- value_proj: bfloat16 [2048, 512], P('fs', 'tp'), may hold values from -1 to 1
- layer_gain: bfloat16 [512], replicated, may hold values from 0.099609375 to 1.8984375
- layer_shift: bfloat16 [512], replicated, may hold values from -3 to 3
- mix_kernel: bfloat16 [4, 128, 128], replicated, may hold values from -0.5 to 0.5
- mix_offset: bfloat16 [4, 128], replicated, may hold values from -4 to 4
- out_proj: bfloat16 [2048, 512], P('fs', 'tp'), may hold values from -0.25 to 0.25
- ffn_gain: bfloat16 [2048], replicated, may hold values from 0.099609375 to 1.8984375
- ffn_gate: bfloat16 [2048, 5632], P('fs', 'tp'), may hold values from -0.125 to 0.125
- ffn_up: bfloat16 [2048, 5632], P('fs', 'tp'), may hold values from -0.125 to 0.125
- ffn_down: bfloat16 [2048, 5632], P('fs', 'tp'), may hold values from -0.078125 to 0.078125
Outputs:
- layer_out: bfloat16 [4096, 2048], P(('rep', 'fs', 'tp'))
All inputs are finite; a program needn't handle non-finite values.
Results may differ from a plain program's by a relative error of at most 0.015.
Values may be sent and summed in bfloat16 or wider, within the bound.
A program may use at most 64 MiB of HBM per device.

v0:
```python
import jax
import jax.numpy as jnp
from jax import lax
from jax.sharding import PartitionSpec as P

epsilon = 1e-06


def rms_norm(rows, gain):
    floats = rows.astype(jnp.float32)
    scale = lax.rsqrt(jnp.mean(floats * floats, axis=-1, keepdims=True) + epsilon)
    return (floats * scale * gain.astype(jnp.float32)).astype(jnp.bfloat16)


def contract_last(left, right):
    return lax.dot_general(
        left, right, (((1,), (1,)), ((), ())), preferred_element_type=jnp.float32
    )


def per_device(
    tokens,
    mix_gain,
    gate_proj,
    value_proj,
    layer_gain,
    layer_shift,
    mix_kernel,
    mix_offset,
    out_proj,
    ffn_gain,
    ffn_gate,
    ffn_up,
    ffn_down,
):
    normed = rms_norm(tokens, mix_gain)
    gate_rows, value_rows, out_rows = (
        lax.all_gather(gate_proj, "fs", axis=0, tiled=True),
        lax.all_gather(value_proj, "fs", axis=0, tiled=True),
        lax.all_gather(out_proj, "fs", axis=0, tiled=True),
    )
    mix_width = layer_gain.shape[0]
    groups = mix_kernel.shape[0]
    span_len = mix_kernel.shape[1]
    causal = jnp.tril(jnp.ones((span_len, span_len), dtype=bool))
    masked = jnp.where(causal[None], mix_kernel, jnp.zeros_like(mix_kernel))
    local_width = gate_rows.shape[1]
    first_col = lax.axis_index("tp") * local_width
    joined = jnp.concatenate([gate_rows, value_rows], axis=1)
    preact = jnp.dot(
        lax.all_gather(normed, "tp", axis=0, tiled=True), joined, preferred_element_type=jnp.float32
    )
    gate_u = jax.nn.gelu(preact[:, :local_width])
    activated = jax.nn.gelu(preact[:, local_width:])
    row_sum, squares = lax.psum(
        (jnp.sum(activated, axis=-1), jnp.sum(activated * activated, axis=-1)), "tp"
    )
    center = (row_sum / mix_width)[:, None]
    spread = (squares / mix_width)[:, None] - center * center
    gain_part = lax.dynamic_slice_in_dim(layer_gain, first_col, local_width).astype(jnp.float32)
    shift_part = lax.dynamic_slice_in_dim(layer_shift, first_col, local_width).astype(jnp.float32)
    values = ((activated - center) * lax.rsqrt(spread + epsilon) * gain_part + shift_part).astype(
        jnp.bfloat16
    )
    group_id = first_col // (mix_width // groups)
    kernel = lax.dynamic_index_in_dim(masked, group_id, 0, keepdims=False)
    offset = lax.dynamic_index_in_dim(mix_offset, group_id, 0, keepdims=False).astype(jnp.float32)
    mixing = jnp.einsum(
        "ts,nsc->ntc",
        kernel,
        values.reshape(-1, span_len, local_width),
        preferred_element_type=jnp.float32,
    )
    mixing = mixing + offset[None, :, None]
    gated_rows = (gate_u * mixing.reshape(gate_u.shape)).astype(jnp.bfloat16)
    mixer_out = lax.psum_scatter(
        contract_last(gated_rows, out_rows).astype(jnp.bfloat16),
        "tp",
        scatter_dimension=0,
        tiled=True,
    ).astype(jnp.float32)
    middle = (tokens.astype(jnp.float32) + mixer_out).astype(jnp.bfloat16)
    normed2 = rms_norm(middle, ffn_gain)
    gathered = lax.all_gather(normed2, "tp", axis=0, tiled=True)
    gate_pre = jnp.dot(
        gathered,
        lax.all_gather(ffn_gate, "fs", axis=0, tiled=True),
        preferred_element_type=jnp.float32,
    )
    up_pre = jnp.dot(
        gathered,
        lax.all_gather(ffn_up, "fs", axis=0, tiled=True),
        preferred_element_type=jnp.float32,
    )
    hidden = (jax.nn.silu(gate_pre) * up_pre).astype(jnp.bfloat16)
    partial_value = contract_last(hidden, lax.all_gather(ffn_down, "fs", axis=0, tiled=True))
    summed = lax.psum_scatter(
        partial_value.astype(jnp.bfloat16), "tp", scatter_dimension=0, tiled=True
    ).astype(jnp.float32)
    return (middle.astype(jnp.float32) + summed).astype(jnp.bfloat16)


def solution(mesh):
    placed = (
        P(("rep", "fs", "tp"), None),
        P(),
        P("fs", "tp"),
        P("fs", "tp"),
        P(),
        P(),
        P(),
        P(),
        P("fs", "tp"),
        P(),
        P("fs", "tp"),
        P("fs", "tp"),
        P("fs", "tp"),
    )
    return jax.shard_map(
        per_device,
        mesh=mesh,
        in_specs=placed,
        out_specs=P(("rep", "fs", "tp"), None),
        check_vma=False,
    )
```

profile of v0, /device:TPU:0, one launch (start us, length us, event | category | flops | bytes accessed | tf_op | source)
XLA Modules:
  0.0 472.7 jit_solution(3375747574779029369)
XLA Ops:
  7.4 0.7 convert_element_type.64
  8.1 1.2 fusion.1
  9.3 2.0 fusion.3
  11.4 0.0 reduce-scatter.3.cloned.1.call-start
  11.5 0.7 bitcast_convert_fusion
  12.2 0.8 dynamic-slice_convert_fusion
  12.9 17.6 %all_gather.25 = bf16[2048,128]{1,0:T(8,128)(2,1)S(1)} all-gather(bf16[512,128]{1,0:T(8,128)(2,1)} %param.15), channel_id=1, replica_groups=mesh['rep'=2,'fs'=4,'tp'=4] {'fs'}, dimensions={0}, use_global_device_ids=true | all-gather | bytes 655360 | tf_op jit(solution)/shard_map/all_gather | solution.py:38
  30.5 16.7 %all_gather.26 = bf16[2048,128]{1,0:T(8,128)(2,1)S(1)} all-gather(bf16[512,128]{1,0:T(8,128)(2,1)S(1)} %copy-done.2), channel_id=1, replica_groups=mesh['rep'=2,'fs'=4,'tp'=4] {'fs'}, dimensions={0}, use_global_device_ids=true | all-gather | bytes 655360 | tf_op jit(solution)/shard_map/all_gather | solution.py:39
  47.2 15.6 %all_gather.27 = bf16[2048,128]{1,0:T(8,128)(2,1)S(1)} all-gather(bf16[512,128]{1,0:T(8,128)(2,1)S(1)} %copy-done.3), channel_id=1, replica_groups=mesh['rep'=2,'fs'=4,'tp'=4] {'fs'}, dimensions={0}, use_global_device_ids=true | all-gather | bytes 655360 | tf_op jit(solution)/shard_map/all_gather | solution.py:40
  62.8 2.3 fusion.9
  65.2 0.2 fusion.37
  65.4 5.7 %all-reduce = (f32[512]{0:T(512)S(1)}, f32[512]{0:T(512)S(1)}) all-reduce(f32[512]{0:T(512)S(1)} %get-tuple-element.6, f32[512]{0:T(512)S(1)} %get-tuple-element.5), channel_id=1, replica_groups=mesh['rep'=2,'fs'=4,'tp'=4] {'tp'}, use_global_device_ids=true, to_apply=%region_4.5 | all-reduce | flops 1024 | bytes 8192 | tf_op jit(solution)/shard_map/psum | solution.py:55
  71.1 0.2 add_convert_fusion
  71.3 0.9 convolution_add_fusion
  72.2 0.1 fusion.21
  72.4 2.1 convolution_convert_fusion
  74.5 0.0 all-gather.10.cloned.1.call-start
  74.5 0.5 all-gather.10.cloned.1.call-update
  75.1 31.4 %reduce-scatter.3.cloned.1.call-done = bf16[128,2048]{1,0:T(8,128)(2,1)} async-done(((bf16[512,2048]{1,0:T(8,128)(2,1)}), bf16[128,2048]{1,0:T(8,128)(2,1)}) %reduce-scatter.3.cloned.1.call-update) | async-done | bytes 524304 | tf_op jit(solution)/shard_map/reduce_scatter | solution.py:76
  106.5 1.3 fusion.5
  107.8 2.0 fusion.7
  109.9 0.0 all-gather.12.cloned.1.call-start
  110.0 0.5 all-gather.12.cloned.1.call-update
  110.6 0.7 all-gather.14.cloned.1.call-update
  111.3 72.6 %all-gather.10.cloned.1.call-done = bf16[2048,1408]{1,0:T(8,128)(2,1)} async-done(((bf16[512,1408]{1,0:T(8,128)(2,1)}), bf16[2048,1408]{1,0:T(8,128)(2,1)}) %all-gather.10.cloned.1.call-update) | async-done | bytes 5767184 | tf_op jit(solution)/shard_map/all_gather | solution.py:87
  183.9 22.1 %all-gather.8.cloned.1.call-done = bf16[512,2048]{1,0:T(8,128)(2,1)} async-done(((bf16[128,2048]{1,0:T(8,128)(2,1)}), bf16[512,2048]{1,0:T(8,128)(2,1)}) %all-gather.8.cloned.1.call-update) | async-done | bytes 2097168 | tf_op jit(solution)/shard_map/all_gather | solution.py:84
  206.0 8.4 %fusion.38 = f32[512,1408]{1,0:T(8,128)} fusion(bf16[512,2048]{1,0:T(8,128)(2,1)} %all-gather.8.cloned.1.call-done, bf16[2048,1408]{1,0:T(8,128)(2,1)} %all-gather.10.cloned.1.call-done), kind=kOutput, calls=%fused_computation.60 | convolution fusion | flops 2952790016 | bytes 10747904 | tf_op jit(solution)/shard_map/dot_general | solution.py:85
  214.4 99.6 %all-gather.12.cloned.1.call-done = bf16[2048,1408]{1,0:T(8,128)(2,1)} async-done(((bf16[512,1408]{1,0:T(8,128)(2,1)}), bf16[2048,1408]{1,0:T(8,128)(2,1)}) %all-gather.12.cloned.1.call-update) | async-done | bytes 5767184 | tf_op jit(solution)/shard_map/all_gather | solution.py:92
  314.0 106.4 %all-gather.14.cloned.1.call-done = bf16[2048,1408]{1,0:T(8,128)(2,1)} async-done(((bf16[512,1408]{1,0:T(8,128)(2,1)}), bf16[2048,1408]{1,0:T(8,128)(2,1)}) %all-gather.14.cloned.1.call-update) | async-done | bytes 5767184 | tf_op jit(solution)/shard_map/all_gather | solution.py:96
  420.5 13.2 %convolution_convert_fusion.1 = bf16[512,2048]{1,0:T(8,128)(2,1)} fusion(bf16[2048,1408]{1,0:T(8,128)(2,1)} %all-gather.14.cloned.1.call-done, bf16[512,2048]{1,0:T(8,128)(2,1)S(1)} %copy-done.5, bf16[2048,1408]{1,0:T(8,128)(2,1)} %all-gather.12.cloned.1.call-done, f32[512,1408]{1,0:T(8,128)} %fusion.38), kind=kOutput, calls=%fused_computation.3 | convolution fusion | flops 5910953984 | bytes 18612224 | tf_op jit(solution)/shard_map/dot_general | solution.py:16
  433.7 29.6 %reduce-scatter.5.cloned.1.call-done = bf16[128,2048]{1,0:T(8,128)(2,1)} async-done(((bf16[512,2048]{1,0:T(8,128)(2,1)}), bf16[128,2048]{1,0:T(8,128)(2,1)}) %reduce-scatter.5.cloned.1.call-update) | async-done | bytes 524304 | tf_op jit(solution)/shard_map/reduce_scatter | solution.py:97
  463.3 2.1 fusion.8
  (26 shorter events, 0.3 us)
Async XLA Ops:
  7.4 23.2 %copy-start.2 = (bf16[512,128]{1,0:T(8,128)(2,1)S(1)}, bf16[512,128]{1,0:T(8,128)(2,1)}, u32[]{:S(2)}) copy-start(bf16[512,128]{1,0:T(8,128)(2,1)} %param.16) | copy-start | bytes 393220
  7.4 39.9 %copy-start.3 = (bf16[512,128]{1,0:T(8,128)(2,1)S(1)}, bf16[512,128]{1,0:T(8,128)(2,1)}, u32[]{:S(2)}) copy-start(bf16[512,128]{1,0:T(8,128)(2,1)} %param.21) | copy-start | bytes 393220
  7.4 55.5 %all-gather.6.cloned.1.call-start = ((), (), s32[]{:S(2)}) async-start(), calls=%async_computation.2 | async-start | bytes 2621440 | tf_op jit(solution)/shard_map/all_gather | solution.py:51
  11.4 95.1 %reduce-scatter.3.cloned.1.call-start = ((), (), s32[]{:S(2)}) async-start(), calls=%async_computation.3 | async-start | bytes 2621440 | tf_op jit(solution)/shard_map/reduce_scatter | solution.py:76
  72.3 2.7 copy-start.4
  72.4 34.2 %copy-start = (bf16[128,2048]{1,0:T(8,128)(2,1)S(1)}, bf16[128,2048]{1,0:T(8,128)(2,1)}, u32[]{:S(2)}) copy-start(bf16[128,2048]{1,0:T(8,128)(2,1)} %param.13) | copy-start | bytes 1572868
  74.5 109.4 %all-gather.10.cloned.1.call-start = ((), (), s32[]{:S(2)}) async-start(), calls=%async_computation.5 | async-start | bytes 7208960 | tf_op jit(solution)/shard_map/all_gather | solution.py:87
  75.0 131.0 %all-gather.8.cloned.1.call-start = ((), (), s32[]{:S(2)}) async-start(), calls=%async_computation.4 | async-start | bytes 2621440 | tf_op jit(solution)/shard_map/all_gather | solution.py:84
  109.9 204.1 %all-gather.12.cloned.1.call-start = ((), (), s32[]{:S(2)}) async-start(), calls=%async_computation.6 | async-start | bytes 7208960 | tf_op jit(solution)/shard_map/all_gather | solution.py:92
  110.5 310.0 %all-gather.14.cloned.1.call-start = ((), (), s32[]{:S(2)}) async-start(), calls=%async_computation.7 | async-start | bytes 7208960 | tf_op jit(solution)/shard_map/all_gather | solution.py:96
  111.2 352.1 %reduce-scatter.5.cloned.1.call-start = ((), (), s32[]{:S(2)}) async-start(), calls=%async_computation.8 | async-start | bytes 2621440 | tf_op jit(solution)/shard_map/reduce_scatter | solution.py:97
  206.0 214.5 %copy-start.5 = (bf16[512,2048]{1,0:T(8,128)(2,1)S(1)}, bf16[512,2048]{1,0:T(8,128)(2,1)}, u32[]{:S(2)}) copy-start(bf16[512,2048]{1,0:T(8,128)(2,1)} %all-gather.8.cloned.1.call-done) | copy-start | bytes 6291460
  214.4 248.9 %copy-start.1 = (bf16[128,2048]{1,0:T(8,128)(2,1)S(1)}, bf16[128,2048]{1,0:T(8,128)(2,1)}, u32[]{:S(2)}) copy-start(bf16[128,2048]{1,0:T(8,128)(2,1)} %reduce-scatter.3.cloned.1.call-done) | copy-start | bytes 1572868
Sparse Core Ops, SparseCore 0:
  11.5 25.2 all-gather.5
  74.6 31.9 reduce-scatter.2
  433.8 29.4 reduce-scatter.4
Sparse Core Ops, SparseCore 1:
  76.5 107.3 all-gather.9
  185.3 20.7 all-gather.7
  207.5 106.5 all-gather.11
  315.6 104.8 all-gather.13
where the time goes:
time: 473 us
  waiting for transfers between devices  364 us (77%)
  blocking collectives  55.5 us (12%)
  matrix products  26.9 us (6%)
  between operations  14.9 us (3%)
  other arithmetic  11.5 us (2%)
    all_gather x1, waiting for transfers between devices, per_device(): lax.all_gather(ffn_down, 'fs', axis=0, tiled=True)  106 us
    all_gather x1, waiting for transfers between devices, per_device(): lax.all_gather(ffn_up, 'fs', axis=0, tiled=True)  99.6 us
    all_gather x1, waiting for transfers between devices, per_device(): lax.all_gather(ffn_gate, 'fs', axis=0, tiled=True)  72.6 us
    reduce_scatter x1, waiting for transfers between devices, per_device(): lax.psum_scatter(contract_last(gated_rows, out_rows).astype(jnp.bfloat16)...  31.4 us
    reduce_scatter x1, waiting for transfers between devices, per_device(): lax.psum_scatter(partial_value.astype(jnp.bfloat16), 'tp', scatter_dimens...  29.6 us
    all_gather x1, waiting for transfers between devices, per_device(): gathered = lax.all_gather(normed2, 'tp', axis=0, tiled=True)  22.1 us
    all_gather x1, blocking collectives, per_device(): lax.all_gather(gate_proj, 'fs', axis=0, tiled=True)  17.6 us
    all_gather x1, blocking collectives, per_device(): lax.all_gather(value_proj, 'fs', axis=0, tiled=True)  16.7 us
  transfers between devices with their start and end apart: 7, of which 6 were waited for; matrix products, arithmetic and copies ran while one was open for 3% of the time, Pallas kernels for 0%

commit v1 on v0

--- a/solution.py
+++ b/solution.py
@@ -4,6 +4,16 @@
 from jax.sharding import PartitionSpec as P
 
 epsilon = 1e-06
+
+
+def gather_around(x, axis, dim):
+    ways, here, step = (lax.axis_size(axis), lax.axis_index(axis), x.shape[dim])
+    lengths = [n * ways if d == dim else n for d, n in enumerate(x.shape)]
+    full = lax.dynamic_update_slice_in_dim(jnp.zeros(lengths, x.dtype), x, here * step, axis=dim)
+    for far in range(1, ways):
+        x = lax.ppermute(x, axis, [(d, (d + 1) % ways) for d in range(ways)])
+        full = lax.dynamic_update_slice_in_dim(full, x, (here - far) % ways * step, axis=dim)
+    return full
 
 
 def rms_norm(rows, gain):
@@ -87,11 +97,7 @@
         lax.all_gather(ffn_gate, "fs", axis=0, tiled=True),
         preferred_element_type=jnp.float32,
     )
-    up_pre = jnp.dot(
-        gathered,
-        lax.all_gather(ffn_up, "fs", axis=0, tiled=True),
-        preferred_element_type=jnp.float32,
-    )
+    up_pre = jnp.dot(gathered, gather_around(ffn_up, "fs", 0), preferred_element_type=jnp.float32)
     hidden = (jax.nn.silu(gate_pre) * up_pre).astype(jnp.bfloat16)
     partial_value = contract_last(hidden, lax.all_gather(ffn_down, "fs", axis=0, tiled=True))
     summed = lax.psum_scatter(

time: 473 us -> 427 us (0.903)
  waiting for transfers between devices: 364 us -> 278 us
  starting transfers between devices: 0.26 us -> 28.6 us
  local copies, waits for them, and re-layouts: 0.03 us -> 10.7 us
    ppermute x0 -> x3, waiting for transfers between devices: none -> 159 us  [gather_around(): x = lax.ppermute(x, axis, [(d, (d + 1) % ways) for d in range(ways)])]
    all_gather x1 -> x0, waiting for transfers between devices: 99.6 us -> none  [per_device(): lax.all_gather(ffn_up, 'fs', axis=0, tiled=True)]
    all_gather x1, waiting for transfers between devices: 72.6 us -> 0.01 us  [per_device(): lax.all_gather(ffn_gate, 'fs', axis=0, tiled=True)]
    all_gather x1, waiting for transfers between devices: 106 us -> 56.9 us  [per_device(): lax.all_gather(ffn_down, 'fs', axis=0, tiled=True)]
    ppermute x0 -> x3, starting transfers between devices: none -> 28.4 us  [gather_around(): x = lax.ppermute(x, axis, [(d, (d + 1) % ways) for d in range(ways)])]
    all_gather x1, waiting for transfers between devices: 22.1 us -> 0.01 us  [per_device(): gathered = lax.all_gather(normed2, 'tp', axis=0, tiled=True)]
    dynamic_update_slice x0 -> x4, local copies, waits for them, and re-layouts: none -> 7.85 us  [the longest x3 6.58 us: gather_around(): lax.dynamic_update_slice_in_dim(full, x, (here - far) % ways * step, axis...]
  transfers between devices with their start and end apart: 7 -> 9, of which waited for: 6 -> 6; matrix products, arithmetic and copies ran while one was open for 3% -> 6% of each run, Pallas kernels for 0% -> 0%
where the time goes in v1:
time: 427 us; the launch traced here: 426 us
  waiting for transfers between devices  278 us (65%)
  blocking collectives  55.5 us (13%)
  starting transfers between devices  28.6 us (7%)
  matrix products  26.9 us (6%)
  between operations  14.9 us (3%)
  other arithmetic  11.5 us (3%)
  local copies, waits for them, and re-layouts  10.7 us (3%)
    ppermute x3, waiting for transfers between devices, gather_around(): x = lax.ppermute(x, axis, [(d, (d + 1) % ways) for d in range(ways)])  159 us
    all_gather x1, waiting for transfers between devices, per_device(): lax.all_gather(ffn_down, 'fs', axis=0, tiled=True)  56.9 us
    reduce_scatter x1, waiting for transfers between devices, per_device(): lax.psum_scatter(contract_last(gated_rows, out_rows).astype(jnp.bfloat16)...  31.4 us
    reduce_scatter x1, waiting for transfers between devices, per_device(): lax.psum_scatter(partial_value.astype(jnp.bfloat16), 'tp', scatter_dimens...  29.7 us
    ppermute x3, starting transfers between devices, gather_around(): x = lax.ppermute(x, axis, [(d, (d + 1) % ways) for d in range(ways)])  28.4 us
    all_gather x1, blocking collectives, per_device(): lax.all_gather(gate_proj, 'fs', axis=0, tiled=True)  17.6 us
    all_gather x1, blocking collectives, per_device(): lax.all_gather(value_proj, 'fs', axis=0, tiled=True)  16.7 us
    all_gather x1, blocking collectives, per_device(): lax.all_gather(out_proj, 'fs', axis=0, tiled=True)  15.6 us
  transfers between devices with their start and end apart: 9, of which 6 were waited for; matrix products, arithmetic and copies ran while one was open for 6% of the time, Pallas kernels for 0%

profile of v1, /device:TPU:0, one launch (start us, length us, event | category | flops | bytes accessed | tf_op | source)
XLA Modules:
  0.0 426.1 jit_solution(9055909583803223131)
XLA Ops:
  7.4 0.7 convert_element_type.64
  8.1 1.2 fusion.1
  9.3 2.0 fusion.3
  11.5 0.7 fusion.35
  12.2 0.8 dynamic-slice_convert_fusion
  12.9 17.6 %all_gather.22 = bf16[2048,128]{1,0:T(8,128)(2,1)S(1)} all-gather(bf16[512,128]{1,0:T(8,128)(2,1)} %param.15), channel_id=1, replica_groups=mesh['rep'=2,'fs'=4,'tp'=4] {'fs'}, dimensions={0}, use_global_device_ids=true | all-gather | bytes 655360 | tf_op jit(solution)/shard_map/all_gather | solution.py:48
  30.5 16.7 %all_gather.23 = bf16[2048,128]{1,0:T(8,128)(2,1)S(1)} all-gather(bf16[512,128]{1,0:T(8,128)(2,1)S(1)} %copy-done.3), channel_id=1, replica_groups=mesh['rep'=2,'fs'=4,'tp'=4] {'fs'}, dimensions={0}, use_global_device_ids=true | all-gather | bytes 655360 | tf_op jit(solution)/shard_map/all_gather | solution.py:49
  47.2 15.6 %all_gather.24 = bf16[2048,128]{1,0:T(8,128)(2,1)S(1)} all-gather(bf16[512,128]{1,0:T(8,128)(2,1)S(1)} %copy-done.4), channel_id=1, replica_groups=mesh['rep'=2,'fs'=4,'tp'=4] {'fs'}, dimensions={0}, use_global_device_ids=true | all-gather | bytes 655360 | tf_op jit(solution)/shard_map/all_gather | solution.py:50
  62.8 2.3 fusion.9
  65.4 5.7 %all-reduce = (f32[512]{0:T(512)S(1)}, f32[512]{0:T(512)S(1)}) all-reduce(f32[512]{0:T(512)S(1)} %get-tuple-element.6, f32[512]{0:T(512)S(1)} %get-tuple-element.5), channel_id=1, replica_groups=mesh['rep'=2,'fs'=4,'tp'=4] {'tp'}, use_global_device_ids=true, to_apply=%region_4.5 | all-reduce | flops 1024 | bytes 8192 | tf_op jit(solution)/shard_map/psum | solution.py:65
  71.3 0.9 convolution_add_fusion
  72.4 2.0 convolution_convert_fusion
  74.5 0.5 all-gather.9.cloned.1.call-update
  75.1 31.4 %reduce-scatter.3.cloned.1.call-done = bf16[128,2048]{1,0:T(8,128)(2,1)} async-done(((bf16[512,2048]{1,0:T(8,128)(2,1)}), bf16[128,2048]{1,0:T(8,128)(2,1)}) %reduce-scatter.3.cloned.1.call-update) | async-done | bytes 524304 | tf_op jit(solution)/shard_map/reduce_scatter | solution.py:86
  106.5 1.3 fusion.5
  107.8 2.0 fusion.7
  109.9 0.5 all-gather.11.cloned.1.call-update
  110.5 1.5 collective-permute-start
  112.1 65.3 %collective-permute-done = bf16[512,1408]{1,0:T(8,128)(2,1)S(1)} collective-permute-done((bf16[512,1408]{1,0:T(8,128)(2,1)S(1)}, bf16[512,1408]{1,0:T(8,128)(2,1)S(1)}, u32[]{:S(2)}, u32[]{:S(2)}) %collective-permute-start) | collective-permute-done | bytes 1441824 | tf_op jit(solution)/shard_map/ppermute | solution.py:14
  177.4 26.8 %collective-permute-start.1 = (bf16[512,1408]{1,0:T(8,128)(2,1)S(1)}, bf16[512,1408]{1,0:T(8,128)(2,1)}, u32[]{:S(2)}, u32[]{:S(2)}) collective-permute-start(bf16[512,1408]{1,0:T(8,128)(2,1)S(1)} %collective-permute-done), channel_id=1, source_target_pairs={{0,4},{4,8},{8,12},{12,0},{1,5},{5,9},{9,13},{13,1},{2,6},{6,10},{... | collective-permute-start | bytes 4325384 | tf_op jit(solution)/shard_map/ppermute | solution.py:14
  204.2 41.2 %collective-permute-done.1 = bf16[512,1408]{1,0:T(8,128)(2,1)} collective-permute-done((bf16[512,1408]{1,0:T(8,128)(2,1)S(1)}, bf16[512,1408]{1,0:T(8,128)(2,1)}, u32[]{:S(2)}, u32[]{:S(2)}) %collective-permute-start.1) | collective-permute-done | bytes 1441824 | tf_op jit(solution)/shard_map/ppermute | solution.py:14
  245.4 2.9 broadcast_in_dim.16
  248.2 1.3 constant_dynamic-update-slice_fusion.3
  249.5 1.2 constant_dynamic-update-slice_fusion.2
  250.7 2.8 constant_dynamic-update-slice_fusion.1
  253.5 52.4 %collective-permute-done.2 = bf16[512,1408]{1,0:T(8,128)(2,1)} collective-permute-done((bf16[512,1408]{1,0:T(8,128)(2,1)}, bf16[512,1408]{1,0:T(8,128)(2,1)}, u32[]{:S(2)}, u32[]{:S(2)}) %collective-permute-start.2) | collective-permute-done | bytes 1441824 | tf_op jit(solution)/shard_map/ppermute | solution.py:14
  305.9 2.6 constant_dynamic-update-slice_fusion
  308.5 8.4 %fusion.40 = f32[512,1408]{1,0:T(8,128)} fusion(bf16[512,2048]{1,0:T(8,128)(2,1)} %all-gather.7.cloned.1.call-done, bf16[2048,1408]{1,0:T(8,128)(2,1)} %all-gather.9.cloned.1.call-done), kind=kOutput, calls=%fused_computation.66 | convolution fusion | flops 2952790016 | bytes 10747904 | tf_op jit(solution)/shard_map/dot_general | solution.py:95
  316.9 56.9 %all-gather.11.cloned.1.call-done = bf16[2048,1408]{1,0:T(8,128)(2,1)} async-done(((bf16[512,1408]{1,0:T(8,128)(2,1)}), bf16[2048,1408]{1,0:T(8,128)(2,1)}) %all-gather.11.cloned.1.call-update) | async-done | bytes 5767184 | tf_op jit(solution)/shard_map/all_gather | solution.py:102
  373.8 13.2 %convolution_convert_fusion.1 = bf16[512,2048]{1,0:T(8,128)(2,1)} fusion(bf16[2048,1408]{1,0:T(8,128)(2,1)} %all-gather.11.cloned.1.call-done, bf16[512,2048]{1,0:T(8,128)(2,1)S(1)} %copy-done.6, bf16[2048,1408]{1,0:T(8,128)(2,1)} %constant_dynamic-update-slice_fusion, f32[512,1408]{1,0:T(8,128)} %fusion.40), kind=kOutput, calls=%fused_computation.3 | convolution fusion | flops 5910953984 | bytes 18612224 | tf_op jit(solution)/shard_map/dot_general | solution.py:26
  387.0 29.7 %reduce-scatter.5.cloned.1.call-done = bf16[128,2048]{1,0:T(8,128)(2,1)} async-done(((bf16[512,2048]{1,0:T(8,128)(2,1)}), bf16[128,2048]{1,0:T(8,128)(2,1)}) %reduce-scatter.5.cloned.1.call-update) | async-done | bytes 524304 | tf_op jit(solution)/shard_map/reduce_scatter | solution.py:103
  416.7 2.1 fusion.8
  (36 shorter events, 0.9 us)
Async XLA Ops:
  7.4 23.2 %copy-start.3 = (bf16[512,128]{1,0:T(8,128)(2,1)S(1)}, bf16[512,128]{1,0:T(8,128)(2,1)}, u32[]{:S(2)}) copy-start(bf16[512,128]{1,0:T(8,128)(2,1)} %param.16) | copy-start | bytes 393220
  7.4 39.9 %copy-start.4 = (bf16[512,128]{1,0:T(8,128)(2,1)S(1)}, bf16[512,128]{1,0:T(8,128)(2,1)}, u32[]{:S(2)}) copy-start(bf16[512,128]{1,0:T(8,128)(2,1)} %param.21) | copy-start | bytes 393220
  7.4 55.5 %all-gather.5.cloned.1.call-start = ((), (), s32[]{:S(2)}) async-start(), calls=%async_computation.2 | async-start | bytes 2621440 | tf_op jit(solution)/shard_map/all_gather | solution.py:61
  11.4 95.1 %reduce-scatter.3.cloned.1.call-start = ((), (), s32[]{:S(2)}) async-start(), calls=%async_computation.3 | async-start | bytes 2621440 | tf_op jit(solution)/shard_map/reduce_scatter | solution.py:86
  72.3 2.7 copy-start.5
  72.3 34.2 %copy-start = (bf16[128,2048]{1,0:T(8,128)(2,1)S(1)}, bf16[128,2048]{1,0:T(8,128)(2,1)}, u32[]{:S(2)}) copy-start(bf16[128,2048]{1,0:T(8,128)(2,1)} %param.13) | copy-start | bytes 1572868
  74.4 36.1 %copy-start.2 = (bf16[512,1408]{1,0:T(8,128)(2,1)S(1)}, bf16[512,1408]{1,0:T(8,128)(2,1)}, u32[]{:S(2)}) copy-start(bf16[512,1408]{1,0:T(8,128)(2,1)} %param.24) | copy-start | bytes 4325380
  74.4 234.0 %all-gather.9.cloned.1.call-start = ((), (), s32[]{:S(2)}) async-start(), calls=%async_computation.5 | async-start | bytes 7208960 | tf_op jit(solution)/shard_map/all_gather | solution.py:97
  75.0 233.5 %all-gather.7.cloned.1.call-start = ((), (), s32[]{:S(2)}) async-start(), calls=%async_computation.4 | async-start | bytes 2621440 | tf_op jit(solution)/shard_map/all_gather | solution.py:94
  109.9 263.9 %all-gather.11.cloned.1.call-start = ((), (), s32[]{:S(2)}) async-start(), calls=%async_computation.6 | async-start | bytes 7208960 | tf_op jit(solution)/shard_map/all_gather | solution.py:102
  110.5 306.2 %reduce-scatter.5.cloned.1.call-start = ((), (), s32[]{:S(2)}) async-start(), calls=%async_computation.7 | async-start | bytes 2621440 | tf_op jit(solution)/shard_map/reduce_scatter | solution.py:103
  110.5 66.8 %collective-permute-start = (bf16[512,1408]{1,0:T(8,128)(2,1)S(1)}, bf16[512,1408]{1,0:T(8,128)(2,1)S(1)}, u32[]{:S(2)}, u32[]{:S(2)}) collective-permute-start(bf16[512,1408]{1,0:T(8,128)(2,1)S(1)} %copy-done.2), channel_id=1, source_target_pairs={{0,4},{4,8},{8,12},{12,0},{1,5},{5,9},{9,13},{13,1},{2,6},{6,10},{... | collective-permute-start | bytes 4325384 | tf_op jit(solution)/shard_map/ppermute | solution.py:14
  177.4 68.0 %collective-permute-start.1 = (bf16[512,1408]{1,0:T(8,128)(2,1)S(1)}, bf16[512,1408]{1,0:T(8,128)(2,1)}, u32[]{:S(2)}, u32[]{:S(2)}) collective-permute-start(bf16[512,1408]{1,0:T(8,128)(2,1)S(1)} %collective-permute-done), channel_id=1, source_target_pairs={{0,4},{4,8},{8,12},{12,0},{1,5},{5,9},{9,13},{13,1},{2,6},{6,10},{... | collective-permute-start | bytes 4325384 | tf_op jit(solution)/shard_map/ppermute | solution.py:14
  245.4 60.5 %collective-permute-start.2 = (bf16[512,1408]{1,0:T(8,128)(2,1)}, bf16[512,1408]{1,0:T(8,128)(2,1)}, u32[]{:S(2)}, u32[]{:S(2)}) collective-permute-start(bf16[512,1408]{1,0:T(8,128)(2,1)} %collective-permute-done.1), channel_id=1, source_target_pairs={{0,4},{4,8},{8,12},{12,0},{1,5},{5,9},{9,13},{13,1},{2,6},{6,10},{... | collective-permute-start | bytes 4325384 | tf_op jit(solution)/shard_map/ppermute | solution.py:14
  308.5 65.3 %copy-start.6 = (bf16[512,2048]{1,0:T(8,128)(2,1)S(1)}, bf16[512,2048]{1,0:T(8,128)(2,1)}, u32[]{:S(2)}) copy-start(bf16[512,2048]{1,0:T(8,128)(2,1)} %all-gather.7.cloned.1.call-done) | copy-start | bytes 6291460
  316.9 99.8 %copy-start.1 = (bf16[128,2048]{1,0:T(8,128)(2,1)S(1)}, bf16[128,2048]{1,0:T(8,128)(2,1)}, u32[]{:S(2)}) copy-start(bf16[128,2048]{1,0:T(8,128)(2,1)} %reduce-scatter.3.cloned.1.call-done) | copy-start | bytes 1572868
Sparse Core Ops, SparseCore 0:
  11.5 25.2 all-gather.4
  74.5 31.9 reduce-scatter.2
  387.1 29.4 reduce-scatter.4
Sparse Core Ops, SparseCore 1:
  76.5 141.8 all-gather.8
  219.8 22.0 all-gather.6
  243.3 130.4 all-gather.10
